TPU v7x, 1024 devices: a whole 4x8x16 slice. The times are simulated.
1024 devices in a mesh: sp: 128 (over z, y), tp: 8 (over x, core).
Axes of the slice: x: 4, y: 8, z: 16, core: 2. Of those that a mesh axis runs over, the one named last changes fastest.
Arguments:
- target: bfloat16 [896, 2048], P('sp'), may hold values from -6 to 6
- source: bfloat16 [32768, 2048], P('sp'), may hold values from -6 to 6
- tgt_gain: float32 [2, 2048], replicated, may hold values from 0.1 to 1.9
- src_gain: float32 [2, 2048], replicated, may hold values from 0.1 to 1.9
- w_query: bfloat16 [2, 2048, 2048], P(None, None, 'tp'), may hold values from -0.125 to 0.125
- w_key: bfloat16 [2, 2048, 2048], P(None, None, 'tp'), may hold values from -0.125 to 0.125
- w_value: bfloat16 [2, 2048, 2048], P(None, None, 'tp'), may hold values from -0.125 to 0.125
- w_out: bfloat16 [2, 2048, 2048], P(None, 'tp'), may hold values from -0.125 to 0.125
- score_scale: float32 [2, 8], P(None, 'tp'), may hold values from 1.5 to 4
Outputs:
- result: bfloat16 [896, 2048], P('sp')
All inputs are finite; a program needn't handle non-finite values.
Results may differ from a plain program's by a relative error of at most 0.015.
Values may be sent and summed in bfloat16 or wider, within the bound.
A program may use at most 64 MiB of HBM per device.

v0:
```python
import math

import jax
import jax.numpy as jnp
from jax import lax
from jax.sharding import Mesh
from jax.sharding import PartitionSpec as P

HEAD_DIM = 256
SP = ("sp_0", "sp_1")


EPS = 1e-06


def joined_along(pieces, dim):
    pieces = jnp.moveaxis(pieces, 0, dim)
    shape = pieces.shape
    return pieces.reshape(*shape[:dim], shape[dim] * shape[dim + 1], *shape[dim + 2 :])


def all_blocks(shard, axes, order):
    pieces = shard
    for k in order:
        pieces = lax.all_gather(pieces, axes[k])
    done = order[::-1]
    back = [done.index(k) for k in range(len(axes))]
    pieces = pieces.transpose(*back, *range(len(axes), pieces.ndim))
    return pieces.reshape(-1, *shard.shape)


def gather_axes(shard, axes, order, dim):
    return joined_along(all_blocks(shard, axes, order), dim)


def summed_rows(shard, axes, dim):
    if not axes:
        return shard
    nearer = lax.psum_scatter(shard, axes[0], scatter_dimension=dim, tiled=True)
    return summed_rows(nearer, axes[1:], dim)


def from_everyone(shard, axis):
    copies = jnp.broadcast_to(shard, (lax.axis_size(axis), *shard.shape))
    return lax.all_to_all(copies, axis, split_axis=0, concat_axis=0, tiled=True)


def over_copies(shard, axis):
    everything = from_everyone(shard, axis)
    return jnp.sum(everything.astype(jnp.float32), axis=0)


def row_scale(values):
    return lax.rsqrt(jnp.mean(values * values, axis=-1, keepdims=True) + EPS)


def head_norm(projected):
    heads = projected.reshape(projected.shape[0], -1, HEAD_DIM)
    heads = heads * row_scale(heads)
    return heads.reshape(projected.shape).astype(jnp.bfloat16)


def source_side(src_float, src_scale, gain_row, key_weight, value_weight):
    normed_src = (src_float * src_scale * gain_row).astype(jnp.bfloat16)
    key_rows = head_norm(jnp.dot(normed_src, key_weight, preferred_element_type=jnp.float32))
    value_rows = jnp.dot(normed_src, value_weight, preferred_element_type=jnp.float32).astype(
        jnp.bfloat16
    )
    return (key_rows, value_rows)


def attend(queries, key_rows, value_rows, scales):
    root = math.sqrt(HEAD_DIM)
    count = queries.shape[0]
    local_heads = scales.shape[0]
    query_heads = queries.reshape(count, local_heads, HEAD_DIM)
    key_heads = key_rows.reshape(key_rows.shape[0], local_heads, HEAD_DIM)
    value_heads = value_rows.reshape(value_rows.shape[0], local_heads, HEAD_DIM)
    scores = jnp.einsum("qhd,khd->hqk", query_heads, key_heads, preferred_element_type=jnp.float32)
    logits = scales[:, None, None] * (scores / root - root)
    weights = jnp.exp(logits)
    denominators = jnp.sum(weights, axis=2).T
    numerators = jnp.einsum(
        "hqk,khd->qhd",
        weights.astype(jnp.bfloat16),
        value_heads,
        preferred_element_type=jnp.float32,
    )
    return (numerators.reshape(count, local_heads * HEAD_DIM), denominators)


def place(terms):
    numer_all = terms[0]
    denom_all = terms[1]
    return (numer_all, denom_all)


def body(target, source, tgt_gain, src_gain, w_query, w_key, w_value, w_out, score_scale):
    local_heads = w_query.shape[2] // HEAD_DIM
    width = local_heads * HEAD_DIM
    tok_rows = target.shape[0]
    layer_count = w_query.shape[0]
    src_float = source.astype(jnp.float32)
    src_scale = row_scale(src_float)
    hidden = target
    for layer_index in range(layer_count):
        key_rows, value_rows = source_side(
            src_float, src_scale, src_gain[layer_index], w_key[layer_index], w_value[layer_index]
        )
        scales = score_scale[layer_index]
        hidden_float = hidden.astype(jnp.float32)
        normed_tgt = (hidden_float * row_scale(hidden_float) * tgt_gain[layer_index]).astype(
            jnp.bfloat16
        )
        weight_now = w_query[layer_index]
        query_rows = head_norm(jnp.dot(normed_tgt, weight_now, preferred_element_type=jnp.float32))
        running = place(
            attend(gather_axes(query_rows, SP, (0, 1), 0), key_rows, value_rows, scales)
        )
        numerators, denominators = (summed_rows(running[0], SP, 0), summed_rows(running[1], SP, 0))
        attended = (
            (numerators.reshape(tok_rows, local_heads, HEAD_DIM) / denominators[:, :, None])
            .reshape(tok_rows, width)
            .astype(jnp.bfloat16)
        )
        share = jnp.dot(attended, w_out[layer_index], preferred_element_type=jnp.float32).astype(
            jnp.bfloat16
        )
        branch = over_copies(share.astype(jnp.float32).astype(jnp.bfloat16), "tp").astype(
            jnp.float32
        )
        hidden = (hidden_float + branch).astype(jnp.bfloat16)
    return hidden


def solution(mesh):
    torus = Mesh(mesh.devices.reshape(16, 8, mesh.shape["tp"]), ("sp_0", "sp_1", "tp"))
    return jax.shard_map(
        body,
        mesh=torus,
        in_specs=(
            P(SP, None),
            P(SP, None),
            P(),
            P(),
            P(None, None, "tp"),
            P(None, None, "tp"),
            P(None, None, "tp"),
            P(None, "tp", None),
            P(None, "tp"),
        ),
        out_specs=P(SP, None),
        check_vma=False,
    )
```

profile of v0, /device:TPU:1, one launch (start us, length us, event | category | flops | bytes accessed | tf_op | source)
XLA Modules:
  0.0 386.2 jit_solution(12815712272280360259)
XLA Ops:
  6.5 0.0 copy-start.3
  6.5 0.0 copy-start.2
  6.5 0.0 copy-start
  6.5 0.0 reduce-scatter.13.cloned.1.call-start
  6.5 1.7 fusion.4
  8.2 0.8 fusion.72
  9.0 2.9 multiply_reduce_fusion.1
  11.9 0.0 copy-start.4
  11.9 0.0 copy-done.3
  12.0 0.0 copy-done.2
  12.0 0.1 fusion.47
  12.1 0.0 copy-done
  12.1 0.4 multiply_reduce_fusion.3
  12.5 0.1 fusion.65
  12.6 36.4 %all-gather.4 = bf16[16,7,256]{2,1,0:T(8,128)(2,1)S(1)} all-gather(bf16[1,7,256]{2,1,0:T(8,128)(2,1)S(1)} %fusion.65), channel_id=2, replica_groups=mesh['sp_0'=16,'sp_1'=8,'tp'=8] {'sp_0'}, dimensions={0}, use_global_device_ids=true | all-gather | bytes 60928 | tf_op jit(solution)/shard_map/all_gather | solution.py:25
  49.0 20.8 %all-gather.1 = bf16[128,7,256]{2,0,1:T(8,128)(2,1)S(1)} all-gather(bf16[16,7,256]{2,0,1:T(8,128)(2,1)S(1)} %copy.26), channel_id=3, replica_groups=mesh['sp_0'=16,'sp_1'=8,'tp'=8] {'sp_1'}, dimensions={0}, use_global_device_ids=true | all-gather | bytes 516096 | tf_op jit(solution)/shard_map/all_gather | solution.py:25
  69.8 0.3 copy.53
  70.0 0.2 reshape.168
  70.2 0.0 copy-done.4
  70.2 0.6 fusion.74
  70.8 2.0 fusion.75
  72.8 3.6 convolution_bitcast_fusion.1
  76.4 0.0 copy-start.1
  76.4 2.5 copy.32
  78.9 0.0 reduce-scatter.13.cloned.1.call-update
  78.9 1.3 dynamic-slice.2
  80.2 1.3 dynamic-slice
  82.8 20.2 %all-reduce.1 = f32[896,1]{0,1:T(1,128)S(1)} all-reduce(f32[896,1]{0,1:T(1,128)S(1)} %transpose.35), channel_id=8, replica_groups=mesh['sp_0'=16,'sp_1'=8,'tp'=8] {'sp_0'}, use_global_device_ids=true, to_apply=%region_7.0.clone | all-reduce | flops 896 | bytes 7168
  103.0 0.1 constant_dynamic-slice_fusion.3
  103.1 0.0 copy-done.1
  103.1 2.6 multiply_reduce_fusion
  105.6 42.2 %reduce-scatter.13.cloned.1.call-done = f32[56,256]{1,0:T(8,128)} async-done(((f32[896,256]{1,0:T(8,128)}), f32[56,256]{1,0:T(8,128)}) %reduce-scatter.13.cloned.1.call-update) | async-done | bytes 57360
  147.8 0.9 copy.33
  148.8 24.6 %all-reduce.7 = (f32[56,256]{0,1:T(8,128)S(1)}, f32[56,1]{0,1:T(1,128)S(1)}) all-reduce(f32[56,256]{0,1:T(8,128)S(1)} %copy.33, f32[56,1]{0,1:T(1,128)S(1)} %constant_dynamic-slice_fusion.3), channel_id=7, replica_groups=mesh['sp_0'=16,'sp_1'=8,'tp'=8] {'sp_1'}, use_global_device_ids=true, to_apply=%region_5.0.clone | all-reduce | flops 14392 | bytes 115136
  173.4 0.1 fusion.69
  173.5 1.6 convolution_convert_fusion.1
  175.0 0.7 broadcast_in_dim.4
  175.8 22.7 %all-to-all-start = ((bf16[8,7,2048]{2,1,0:T(8,128)(2,1)}), bf16[8,7,2048]{2,1,0:T(8,128)(2,1)S(1)}, u32[]{:S(2)}, u32[]{:S(2)}) async-start(bf16[8,7,2048]{2,1,0:T(8,128)(2,1)} %broadcast_in_dim.4), calls=%async_computation | async-start | bytes 524288 | tf_op jit(solution)/shard_map/all_to_all | solution.py:45
  198.4 0.0 reduce-scatter.15.cloned.1.call-start
  198.4 6.5 %all-to-all-done = bf16[8,7,2048]{2,1,0:T(8,128)(2,1)S(1)} async-done(((bf16[8,7,2048]{2,1,0:T(8,128)(2,1)}), bf16[8,7,2048]{2,1,0:T(8,128)(2,1)S(1)}, u32[]{:S(2)}, u32[]{:S(2)}) %all-to-all-start) | async-done | bytes 229408 | tf_op jit(solution)/shard_map/all_to_all | solution.py:45
  204.9 0.3 convert_reduce_fusion.1
  205.2 0.1 fusion.51
  205.3 0.4 multiply_reduce_fusion.2
  205.7 0.0 copy-start.5
  205.8 0.1 fusion.66
  205.8 20.3 %all-gather.5 = bf16[16,7,256]{2,1,0:T(8,128)(2,1)S(1)} all-gather(bf16[1,7,256]{2,1,0:T(8,128)(2,1)S(1)} %fusion.66), channel_id=4, replica_groups=mesh['sp_0'=16,'sp_1'=8,'tp'=8] {'sp_0'}, dimensions={0}, use_global_device_ids=true | all-gather | bytes 60928 | tf_op jit(solution)/shard_map/all_gather | solution.py:25
  226.2 19.3 %all-gather.3 = bf16[128,7,256]{2,0,1:T(8,128)(2,1)S(1)} all-gather(bf16[16,7,256]{2,0,1:T(8,128)(2,1)S(1)} %copy.29), channel_id=5, replica_groups=mesh['sp_0'=16,'sp_1'=8,'tp'=8] {'sp_1'}, dimensions={0}, use_global_device_ids=true | all-gather | bytes 516096 | tf_op jit(solution)/shard_map/all_gather | solution.py:25
  245.5 0.3 copy.52
  245.8 0.2 reshape.170
  245.9 0.0 copy-done.5
  245.9 1.1 fusion.76
  247.0 2.3 convolution_bitcast_fusion
  249.3 1.2 copy.40
  250.5 0.0 reduce-scatter.15.cloned.1.call-update
  250.6 21.7 %all-reduce.4 = f32[896,1]{0,1:T(1,128)S(1)} all-reduce(f32[896,1]{0,1:T(1,128)S(1)} %transpose.38), channel_id=12, replica_groups=mesh['sp_0'=16,'sp_1'=8,'tp'=8] {'sp_0'}, use_global_device_ids=true, to_apply=%region_16.0.clone | all-reduce | flops 896 | bytes 7168
  272.3 0.1 constant_dynamic-slice_fusion.1
  272.3 49.9 %reduce-scatter.15.cloned.1.call-done = f32[56,256]{1,0:T(8,128)} async-done(((f32[896,256]{1,0:T(8,128)}), f32[56,256]{1,0:T(8,128)}) %reduce-scatter.15.cloned.1.call-update) | async-done | bytes 57360
  322.2 0.9 copy.41
  323.1 24.7 %all-reduce.6 = (f32[56,256]{0,1:T(8,128)S(1)}, f32[56,1]{0,1:T(1,128)S(1)}) all-reduce(f32[56,256]{0,1:T(8,128)S(1)} %copy.41, f32[56,1]{0,1:T(1,128)S(1)} %constant_dynamic-slice_fusion.1), channel_id=11, replica_groups=mesh['sp_0'=16,'sp_1'=8,'tp'=8] {'sp_1'}, use_global_device_ids=true, to_apply=%region_14.0.clone | all-reduce | flops 14392 | bytes 115136
  347.8 0.1 fusion.70
  347.9 1.6 convolution_convert_fusion
  349.5 29.0 %all_to_all.10 = bf16[8,7,2048]{2,1,0:T(8,128)(2,1)S(1)} all-to-all(bf16[8,7,2048]{2,1,0:T(8,128)(2,1)S(1)} %broadcast_in_dim.5), channel_id=1, replica_groups=mesh['sp_0'=16,'sp_1'=8,'tp'=8] {'tp'}, dimensions={0} | all-to-all | bytes 458752 | tf_op jit(solution)/shard_map/all_to_all | solution.py:45
  378.5 0.3 convert_reduce_fusion
  378.8 0.6 fusion.54
  (13 shorter events, 0.1 us)
Async XLA Ops:
  6.5 5.4 %copy-start.3 = (f32[2,2048]{1,0:T(2,128)S(1)}, f32[2,2048]{1,0:T(2,128)}, u32[]{:S(2)}) copy-start(f32[2,2048]{1,0:T(2,128)} %param.11) | copy-start | bytes 49156
  6.5 5.4 %copy-start.2 = (bf16[7,2048]{1,0:T(8,128)(2,1)S(1)}, bf16[7,2048]{1,0:T(8,128)(2,1)}, u32[]{:S(2)}) copy-start(bf16[7,2048]{1,0:T(8,128)(2,1)} %param.9) | copy-start | bytes 86020
  6.5 5.6 %copy-start = (bf16[2,2048,256]{2,1,0:T(8,128)(2,1)S(1)}, bf16[2,2048,256]{2,1,0:T(8,128)(2,1)}, u32[]{:S(2)}) copy-start(bf16[2,2048,256]{2,1,0:T(8,128)(2,1)} %param.13) | copy-start | bytes 6291460
  6.5 141.3 %reduce-scatter.13.cloned.1.call-start = ((), (), s32[]{:S(2)}) async-start(), calls=%async_computation.4 | async-start | bytes 974848
  11.9 58.3 %copy-start.4 = (f32[2,1]{0,1:T(1,128)S(1)}, f32[2,1]{0,1:T(1,128)}, u32[]{:S(2)}) copy-start(f32[2,1]{0,1:T(1,128)} %param.17) | copy-start | bytes 28
  76.4 26.7 %copy-start.1 = (bf16[256,2048]{1,0:T(8,128)(2,1)S(1)}, bf16[256,2048]{1,0:T(8,128)(2,1)}, u32[]{:S(2)}) copy-start(bf16[256,2048]{1,0:T(8,128)(2,1)} %param.10) | copy-start | bytes 3145732
  175.8 29.1 %all-to-all-start = ((bf16[8,7,2048]{2,1,0:T(8,128)(2,1)}), bf16[8,7,2048]{2,1,0:T(8,128)(2,1)S(1)}, u32[]{:S(2)}, u32[]{:S(2)}) async-start(bf16[8,7,2048]{2,1,0:T(8,128)(2,1)} %broadcast_in_dim.4), calls=%async_computation | async-start | bytes 524288 | tf_op jit(solution)/shard_map/all_to_all | solution.py:45
  198.4 123.8 %reduce-scatter.15.cloned.1.call-start = ((), (), s32[]{:S(2)}) async-start(), calls=%async_computation.5 | async-start | bytes 974848
  205.7 40.2 %copy-start.5 = (f32[256,256]{0,1:T(8,128)S(1)}, f32[256,256]{0,1:T(8,128)}, u32[]{:S(2)}) copy-start(f32[256,256]{0,1:T(8,128)} %get-tuple-element.26) | copy-start | bytes 786436
Sparse Core Ops, SparseCore 0:
  79.0 68.7 reduce-scatter.12
  250.7 71.4 reduce-scatter.14
where the time goes:
time: 387 us; the launch traced here: 386 us
  blocking collectives  217 us (56%)
  waiting for transfers between devices  98.6 us (25%)
  starting transfers between devices  22.7 us (6%)
  matrix products  18.3 us (5%)
  between operations  14.9 us (4%)
  local copies, waits for them, and re-layouts  11.5 us (3%)
    all_gather x4, blocking collectives, all_blocks(): pieces = lax.all_gather(pieces, axes[k])  96.8 us
    unnamed x4, waiting for transfers between devices  92.1 us
    unnamed x4, blocking collectives  91.2 us
    all_to_all x1, blocking collectives, from_everyone(): return lax.all_to_all(copies, axis, split_axis=0, concat_axis=0, tiled=True)  29 us
    all_to_all x1, starting transfers between devices, from_everyone(): return lax.all_to_all(copies, axis, split_axis=0, concat_axis=0, tiled=True)  22.7 us
    unnamed x20, local copies, waits for them, and re-layouts  8.35 us
  transfers between devices with their start and end apart: 3, of which 3 were waited for; matrix products, arithmetic and copies ran while one was open for 1% of the time, Pallas kernels for 0%

commit v1 on v0

v1 whole, which is shorter than its diff:
```python
import functools
import math

import jax
import jax.numpy as jnp
from jax import lax
from jax.experimental import pallas as pl
from jax.experimental.pallas import tpu as pltpu
from jax.sharding import Mesh
from jax.sharding import PartitionSpec as P

HEAD_DIM = 256
ROOT = math.sqrt(HEAD_DIM)
EPS = 1e-06
PAD = 8
MESH = pl.DeviceIdType.MESH
BF16 = jnp.bfloat16
F32 = jnp.float32


def row_scale(values):
    return lax.rsqrt(jnp.mean(values * values, axis=-1, keepdims=True) + EPS)


def dot_nt(a, b):
    return lax.dot_general(a, b, (((1,), (1,)), ((), ())), preferred_element_type=F32)


def kernel(
    sizes,
    target,
    source,
    tgt_gain,
    src_gain,
    w_query,
    w_key,
    w_value,
    w_out,
    score_scale,
    out,
    hid,
    src,
    tgt,
    tgain,
    sgain,
    wq,
    wk,
    wv,
    wo,
    scl,
    ns,
    kv,
    qall,
    nacc,
    dacc,
    nsend,
    nrecv,
    share,
    load_sem,
    kv_send,
    kv_recv,
    q_send,
    q_recv,
    n_send,
    n_recv,
    t_send,
    t_recv,
):
    nz, ny, nt = sizes
    half = ny // 2
    z, y, t = lax.axis_index("z"), lax.axis_index("y"), lax.axis_index("tp")
    layers = wq.shape[0]
    rows = src.shape[0]
    toks = target.shape[0]
    tall = nz * PAD

    loads = [
        pltpu.make_async_copy(a, b, load_sem.at[i])
        for i, (a, b) in enumerate(
            [
                (source, src),
                (src_gain, sgain),
                (w_key.at[0], wk.at[0]),
                (w_value.at[0], wv.at[0]),
                (target, tgt),
                (tgt_gain, tgain),
                (score_scale, scl),
                (w_query.at[0], wq.at[0]),
                (w_key.at[1], wk.at[1]),
                (w_value.at[1], wv.at[1]),
                (w_out.at[0], wo.at[0]),
                (w_query.at[1], wq.at[1]),
                (w_out.at[1], wo.at[1]),
            ]
        )
    ]
    for load in loads:
        load.start()

    barrier = pltpu.get_barrier_semaphore()
    right, left = lax.rem(y + 1, ny), lax.rem(y + ny - 1, ny)

    def greet_z(k, carry):
        pl.semaphore_signal(barrier, inc=1, device_id={"z": lax.rem(z + k, nz)}, device_id_type=MESH)
        return carry

    def greet_t(k, carry):
        pl.semaphore_signal(barrier, inc=1, device_id={"tp": lax.rem(t + k, nt)}, device_id_type=MESH)
        return carry

    lax.fori_loop(1, nz, greet_z, 0)
    pl.semaphore_signal(barrier, inc=1, device_id={"y": right}, device_id_type=MESH)
    pl.semaphore_signal(barrier, inc=1, device_id={"y": left}, device_id_type=MESH)
    lax.fori_loop(1, nt, greet_t, 0)

    loads[0].wait()
    loads[1].wait()
    step = 16

    def norm_rows(i, carry):
        at = pl.ds(pl.multiple_of(i * step, step), step)
        x = src[at, :].astype(F32)
        x = x * row_scale(x)
        for layer in range(layers):
            ns[layer, at, :] = (x * sgain[layer : layer + 1, :]).astype(BF16)
        return carry

    lax.fori_loop(0, rows // step, norm_rows, 0)

    def source_side(layer):
        normed = ns[layer]
        keys = jnp.dot(normed, wk[layer], preferred_element_type=F32)
        kv[layer, 0, 0] = (keys * row_scale(keys)).astype(BF16)
        kv[layer, 1, 0] = jnp.dot(normed, wv[layer], preferred_element_type=F32).astype(BF16)

    def queries_of(layer):
        hidden = hid[...]
        normed = (hidden * row_scale(hidden) * tgain[layer : layer + 1, :]).astype(BF16)
        queries = jnp.dot(normed, wq[layer], preferred_element_type=F32)
        qall[layer, 0] = (queries * row_scale(queries)).astype(BF16)

    loads[2].wait()
    loads[3].wait()
    source_side(0)
    for i in (4, 5, 6, 7):
        loads[i].wait()
    hid[...] = jnp.zeros_like(hid)
    hid[0:toks, :] = tgt[...].astype(F32)
    queries_of(0)
    loads[8].wait()
    loads[9].wait()
    source_side(1)
    for i in (10, 11, 12):
        loads[i].wait()

    pl.semaphore_wait(barrier, nz - 1 + 2 + nt - 1)

    def ring(layer, which, step):
        copies = []
        for way, peer in ((0, right), (1, left)):
            if step == half - 1 and which != way:
                continue
            held = 0 if step == 0 else (step if way == 0 else half + step)
            lands = half if step == half - 1 else (step + 1 if way == 0 else half + step + 1)
            copies.append(
                pltpu.make_async_remote_copy(
                    src_ref=kv.at[layer, which, held],
                    dst_ref=kv.at[layer, which, lands],
                    send_sem=kv_send.at[layer, which, way, step],
                    recv_sem=kv_recv.at[layer, which, lands],
                    device_id={"y": peer},
                    device_id_type=MESH,
                )
            )
        return copies

    def ring_start(layer, which, step):
        for copy in ring(layer, which, step):
            copy.start()

    def ring_arrived(layer, which, step):
        for copy in ring(layer, which, step):
            copy.wait_recv()

    def ring_next(layer, which, step):
        ring_arrived(layer, which, step)
        if step < half - 1:
            for copy in ring(layer, which, step + 1):
                copy.start()

    def far_first(k):
        return k

    def z_order(i):
        away = (i + 1) // 2
        side = lax.rem(i, 2)
        return nz // 2 + jnp.where(side == 1, away, -away)

    def q_copy(layer, k):
        return pltpu.make_async_remote_copy(
            src_ref=qall.at[layer, 0],
            dst_ref=qall.at[layer, nz - k],
            send_sem=q_send.at[layer],
            recv_sem=q_recv.at[layer],
            device_id={"z": lax.rem(z + k, nz)},
            device_id_type=MESH,
        )

    def q_start(layer):
        def go(i, carry):
            q_copy(layer, z_order(i)).start()
            return carry

        lax.fori_loop(0, nz - 1, go, 0)

    def wait_all(ref, send, recv):
        both = pltpu.make_async_remote_copy(
            src_ref=ref,
            dst_ref=ref,
            send_sem=send,
            recv_sem=recv,
            device_id={"z": lax.rem(z + 1, nz)},
            device_id_type=MESH,
        )
        both.wait_recv()
        return both

    def n_start(layer):
        def go(i, carry):
            k = z_order(i)
            pltpu.make_async_remote_copy(
                src_ref=nsend.at[layer, k],
                dst_ref=nrecv.at[layer, nz - k],
                send_sem=n_send.at[layer],
                recv_sem=n_recv.at[layer],
                device_id={"z": lax.rem(z + k, nz)},
                device_id_type=MESH,
            ).start()
            return carry

        lax.fori_loop(0, nz - 1, go, 0)

    def attend(layer, slot):
        scores = dot_nt(qall[layer].reshape(tall, HEAD_DIM), kv[layer, 0, slot])
        weights = jnp.exp(scl[layer : layer + 1, :] * (scores * (1.0 / ROOT) - ROOT))
        sums = weights[:, 0:128]
        for c in range(128, rows, 128):
            sums = sums + weights[:, c : c + 128]
        dacc[...] += sums
        nacc[...] += jnp.dot(weights.astype(BF16), kv[layer, 1, slot], preferred_element_type=F32)

    def partials(layer):
        denoms = jnp.sum(dacc[...].T, axis=0, keepdims=True)
        upper = denoms.astype(BF16).astype(F32)
        lower = denoms - upper
        pad = jnp.zeros((1, 128 - tall), F32)
        parts = [upper, lower] if tall == 128 else [upper, pad, lower, pad]
        extra = jnp.concatenate(parts, axis=1).reshape(1, 1, 256)
        shape = (nz, PAD, HEAD_DIM)
        lane = lax.rem(lax.broadcasted_iota(jnp.int32, shape, 2), 128)
        block = lax.broadcasted_iota(jnp.int32, shape, 0)
        row = lax.broadcasted_iota(jnp.int32, shape, 1)
        mine = jnp.where(lane // PAD == block, jnp.broadcast_to(extra, shape), 0.0)
        full = jnp.where(row == PAD - 1, mine, nacc[...].reshape(shape)).astype(BF16)
        nsend[layer] = full
        nrecv[layer, 0] = full[0]

    def share_of(layer):
        total = jnp.sum(nrecv[layer].astype(F32), axis=0)
        shape = (PAD, 128)
        lane = lax.broadcasted_iota(jnp.int32, shape, 1)
        row = lax.broadcasted_iota(jnp.int32, shape, 0)
        both = total[PAD - 1 : PAD, 0:128] + total[PAD - 1 : PAD, 128:256]
        denoms = jnp.sum(
            jnp.where(lax.rem(lane, PAD) == row, jnp.broadcast_to(both, shape), 0.0),
            axis=1,
            keepdims=True,
        )
        real = lax.broadcasted_iota(jnp.int32, (PAD, HEAD_DIM), 0) < toks
        attended = jnp.where(real, total / denoms, 0.0).astype(BF16)
        share[layer, 0] = jnp.dot(attended, wo[layer], preferred_element_type=F32).astype(BF16)

    def t_copy(layer, k):
        return pltpu.make_async_remote_copy(
            src_ref=share.at[layer, 0],
            dst_ref=share.at[layer, nt - k],
            send_sem=t_send.at[layer],
            recv_sem=t_recv.at[layer],
            device_id={"tp": lax.rem(t + k, nt)},
            device_id_type=MESH,
        )

    def t_start(layer):
        for k in sorted(range(1, nt), key=lambda k: abs(k - nt // 2)):
            t_copy(layer, k).start()

    def add_branch(layer):
        branch = share[layer, 0].astype(F32)
        for k in range(1, nt):
            branch = branch + share[layer, k].astype(F32)
        return (hid[...] + branch).astype(BF16)

    def clear():
        nacc[...] = jnp.zeros_like(nacc)
        dacc[...] = jnp.zeros_like(dacc)

    q_start(0)
    ring_start(0, 0, 0)
    ring_start(0, 1, 0)
    clear()
    waits = []
    for s in range(half):
        ring_next(0, 0, s)
        ring_next(0, 1, s)
        if s == half - 2:
            ring_start(1, 0, 0)
            ring_start(1, 1, 0)
        if s == 0:
            waits.append(wait_all(qall.at[0, pl.ds(1, nz - 1)], q_send.at[0], q_recv.at[0]))
            attend(0, 0)
        if s < half - 1:
            attend(0, s + 1)
            attend(0, half + s + 1)
        else:
            attend(0, half)
    partials(0)
    n_start(0)
    ring_next(1, 0, 0)
    ring_next(1, 1, 0)
    waits.append(wait_all(nrecv.at[0, pl.ds(1, nz - 1)], n_send.at[0], n_recv.at[0]))
    share_of(0)
    t_start(0)
    ring_next(1, 0, 1)
    ring_next(1, 1, 1)
    waits.append(wait_all(share.at[0, pl.ds(1, nt - 1)], t_send.at[0], t_recv.at[0]))
    hid[...] = add_branch(0).astype(F32)
    queries_of(1)
    q_start(1)
    clear()
    for s in range(2, half):
        ring_next(1, 0, s)
        ring_next(1, 1, s)
    waits.append(wait_all(qall.at[1, pl.ds(1, nz - 1)], q_send.at[1], q_recv.at[1]))

    def attend_slot(slot, carry):
        attend(1, slot)
        return carry

    lax.fori_loop(0, ny, attend_slot, 0)
    partials(1)
    n_start(1)
    waits.append(wait_all(nrecv.at[1, pl.ds(1, nz - 1)], n_send.at[1], n_recv.at[1]))
    share_of(1)
    t_start(1)
    waits.append(wait_all(share.at[1, pl.ds(1, nt - 1)], t_send.at[1], t_recv.at[1]))
    out[...] = add_branch(1)[0:toks, :]

    for both in waits:
        both.wait_send()
    for layer in range(layers):
        for s in range(half):
            for which in (0, 1):
                for copy in ring(layer, which, s):
                    copy.wait_send()


def body(sizes, *arrays):
    target, source = arrays[0], arrays[1]
    w_query, w_out = arrays[4], arrays[7]
    nz, ny, nt = sizes
    toks, width = target.shape
    rows = source.shape[0]
    layers = w_query.shape[0]
    half = ny // 2
    hbm = pl.BlockSpec(memory_space=pl.ANY)
    vmem = pltpu.VMEM
    dma = pltpu.SemaphoreType.DMA
    return pl.pallas_call(
        functools.partial(kernel, sizes),
        out_shape=jax.ShapeDtypeStruct((toks, width), BF16),
        in_specs=[hbm] * 9,
        out_specs=pl.BlockSpec(memory_space=pltpu.VMEM),
        scratch_shapes=[
            vmem((PAD, width), F32),
            vmem((rows, width), BF16),
            vmem((toks, width), BF16),
            vmem((layers, width), F32),
            vmem((layers, width), F32),
            vmem((layers, width, HEAD_DIM), BF16),
            vmem((layers, width, HEAD_DIM), BF16),
            vmem((layers, width, HEAD_DIM), BF16),
            vmem((layers, HEAD_DIM, width), BF16),
            vmem((layers, 1), F32),
            vmem((layers, rows, width), BF16),
            vmem((layers, 2, ny, rows, HEAD_DIM), BF16),
            vmem((layers, nz, PAD, HEAD_DIM), BF16),
            vmem((nz * PAD, HEAD_DIM), F32),
            vmem((nz * PAD, 128), F32),
            vmem((layers, nz, PAD, HEAD_DIM), BF16),
            vmem((layers, nz, PAD, HEAD_DIM), BF16),
            vmem((layers, nt, PAD, width), BF16),
            dma((13,)),
            dma((layers, 2, 2, half)),
            dma((layers, 2, ny)),
            dma((layers,)),
            dma((layers,)),
            dma((layers,)),
            dma((layers,)),
            dma((layers,)),
            dma((layers,)),
        ],
        compiler_params=pltpu.CompilerParams(collective_id=0, has_side_effects=True),
    )(*arrays)


SP = ("z", "y")


def torus_of(mesh):
    return Mesh(mesh.devices.reshape(16, 8, mesh.shape["tp"]), ("z", "y", "tp"))


def on_torus(torus):
    sizes = tuple(torus.shape[a] for a in ("z", "y", "tp"))
    return jax.shard_map(
        functools.partial(body, sizes),
        mesh=torus,
        in_specs=(
            P(SP, None),
            P(SP, None),
            P(),
            P(),
            P(None, None, "tp"),
            P(None, None, "tp"),
            P(None, None, "tp"),
            P(None, "tp", None),
            P(None, "tp"),
        ),
        out_specs=P(SP, None),
        check_vma=False,
    )


def solution(mesh):
    return on_torus(torus_of(mesh))
```

time: 387 us -> 88.9 us (0.23)
  blocking collectives: 217 us -> 0 us
  waiting for transfers between devices: 98.6 us -> 0 us
  Pallas kernels: 0 us -> 86 us
  starting transfers between devices: 22.7 us -> 0 us
  matrix products: 18.3 us -> 0 us
  between operations: 14.9 us -> 0.01 us
  local copies, waits for them, and re-layouts: 11.5 us -> 2.67 us
    all_gather x4 -> x0, blocking collectives: 96.8 us -> none  [all_blocks(): pieces = lax.all_gather(pieces, axes[k])]
    unnamed x4 -> x0, waiting for transfers between devices: 92.1 us -> none
    unnamed x4 -> x0, blocking collectives: 91.2 us -> none
    pallas_call x0 -> x1, Pallas kernels: none -> 86 us  [body(): pl.pallas_call(functools.partial(kernel, sizes), out_shape=jax.ShapeDtype...]
    all_to_all x1 -> x0, blocking collectives: 29 us -> none  [from_everyone(): return lax.all_to_all(copies, axis, split_axis=0, concat_axis=0, tiled=True)]
    all_to_all x1 -> x0, starting transfers between devices: 22.7 us -> none  [from_everyone(): return lax.all_to_all(copies, axis, split_axis=0, concat_axis=0, tiled=True)]
    dot_general x10 -> x0, matrix products: 18.3 us -> none  [the longest x2 5.85 us: attend(): jnp.einsum('hqk,khd->qhd', weights.astype(jnp.bfloat16), value_heads, pre...]
    all_to_all x1 -> x0, waiting for transfers between devices: 6.46 us -> none  [from_everyone(): return lax.all_to_all(copies, axis, split_axis=0, concat_axis=0, tiled=True)]
  transfers between devices with their start and end apart: 3 -> 0, of which waited for: 3 -> 0; matrix products, arithmetic and copies ran while one was open for 1% -> 0% of each run, Pallas kernels for 0% -> 0%
where the time goes in v1:
time: 88.9 us; the launch traced here: 88.7 us
  Pallas kernels  86 us (97%)
  local copies, waits for them, and re-layouts  2.67 us (3%)
    pallas_call x1, Pallas kernels, body(): pl.pallas_call(functools.partial(kernel, sizes), out_shape=jax.ShapeDtype...  86 us
    unnamed x2, local copies, waits for them, and re-layouts  2.67 us

profile of v1, /device:TPU:1, one launch (start us, length us, event | category | flops | bytes accessed | tf_op | source)
XLA Modules:
  0.0 88.7 jit_solution(9658153217675203497)
XLA Ops:
  0.0 1.3 %copy.10.score_scale = f32[2,1]{1,0:T(2,128)} copy(f32[2,1]{0,1:T(1,128)} %param.17) | data formatting | bytes 16 | tf_op args[8]
  1.3 86.0 %shard_map.91 = bf16[7,2048]{1,0:T(8,128)(2,1)} custom-call(bf16[7,2048]{1,0:T(8,128)(2,1)} %target.1, bf16[256,2048]{1,0:T(8,128)(2,1)} %source.1, f32[2,2048]{1,0:T(2,128)} %tgt_gain.1, f32[2,2048]{1,0:T(2,128)} %src_gain.1, bf16[2,2048,256]{2,1,0:T(8,128)(2,1)} %w_query.1, bf16[2,2048,256]{2,1,0:T(8,128)(2,1)} %w_key.1, bf16[2,2048,256]{2,1,0:T(8,128)(2,1)} %w_value.1, ...), custom_call_target="tpu_custom_call" | custom-call | tf_op jit(solution)/shard_map/pallas_call | solution.py:378
  87.3 1.4 %copy.12 = bf16[7,2048]{1,0:T(8,128)(2,1)} copy(bf16[7,2048]{1,0:T(8,128)(2,1)} %shard_map.91) | data formatting | bytes 57344

commit v2 on v1

v2 whole, which is shorter than its diff:
```python
import functools
import math

import jax
import jax.numpy as jnp
from jax import lax
from jax.experimental import pallas as pl
from jax.experimental.pallas import tpu as pltpu
from jax.sharding import Mesh
from jax.sharding import PartitionSpec as P

HEAD_DIM = 256
ROOT = math.sqrt(HEAD_DIM)
EPS = 1e-06
PAD = 8
MESH = pl.DeviceIdType.MESH
scope = jax.named_scope
BF16 = jnp.bfloat16
F32 = jnp.float32


def row_scale(values):
    return lax.rsqrt(jnp.mean(values * values, axis=-1, keepdims=True) + EPS)


def dot_nt(a, b):
    return lax.dot_general(a, b, (((1,), (1,)), ((), ())), preferred_element_type=F32)


def kernel(
    sizes,
    target,
    source,
    tgt_gain,
    src_gain,
    w_query,
    w_key,
    w_value,
    w_out,
    score_scale,
    out,
    hid,
    src,
    scale_of,
    tgt,
    tgain,
    sgain,
    wq,
    wk,
    wv,
    wo,
    scl,
    ns,
    kv0,
    kv1,
    q0,
    q1,
    nsend0,
    nrecv0,
    nsend1,
    nrecv1,
    share,
    load_sem,
    kv0_send,
    kv0_recv,
    kv1_send,
    kv1_recv,
    q_send,
    q_recv,
    n_send,
    n_recv,
    t_send,
    t_recv,
):
    nz, ny, nt = sizes
    half = ny // 2
    z, y, t = lax.axis_index("z"), lax.axis_index("y"), lax.axis_index("tp")
    layers = wq.shape[0]
    rows = src.shape[0]
    toks = target.shape[0]
    tall = nz * PAD

    def line(dy):
        return lax.rem(y + (dy + ny), ny)

    def plane(k):
        return lax.rem(z + k, nz)

    def load(i, a, b):
        return pltpu.make_async_copy(a, b, load_sem.at[i])

    first = [
        load(0, source, src),
        load(1, src_gain, sgain),
        load(2, w_key.at[0], wk.at[0]),
        load(3, w_value.at[0], wv.at[0]),
    ]
    later = [
        load(4, target, tgt),
        load(5, tgt_gain, tgain),
        load(6, w_query.at[0], wq.at[0]),
        load(7, score_scale, scl),
        load(8, w_key.at[1], wk.at[1]),
        load(9, w_value.at[1], wv.at[1]),
        load(10, w_out.at[0], wo.at[0]),
        load(11, w_query.at[1], wq.at[1]),
        load(12, w_out.at[1], wo.at[1]),
    ]
    for one in first:
        one.start()

    barrier = pltpu.get_barrier_semaphore()

    def greet(peer):
        pl.semaphore_signal(barrier, inc=1, device_id=peer, device_id_type=MESH)

    sides = (2, -2)
    for dy in (1, -1) + sides:
        greet({"y": line(dy)})
    for k in range(1, nt):
        greet({"tp": lax.rem(t + k, nt)})

    def greet_planes(k, carry):
        greet({"z": plane(k)})
        for dy in sides:
            greet({"z": plane(k), "y": line(dy)})
        return carry

    lax.fori_loop(1, nz, greet_planes, 0)
    greeted = 4 + nt - 1 + (nz - 1) * 3
    for one in later:
        one.start()

    step = 16

    def at_rows(i):
        return pl.ds(pl.multiple_of(i * step, step), step)

    def squares(i, carry):
        for u in range(2):
            x = src[at_rows(2 * i + u), :].astype(F32)
            x = x * x
            total = x[:, 0:128]
            for c in range(128, x.shape[1], 128):
                total = total + x[:, c : c + 128]
            scale_of[at_rows(2 * i + u), :] = total
        return carry

    def norm_rows(layer):
        def go(i, carry):
            for u in range(2):
                at = at_rows(2 * i + u)
                x = src[at, :].astype(F32) * scale_of[at, 0:1]
                ns[at, :] = (x * sgain[layer : layer + 1, :]).astype(BF16)
            return carry

        lax.fori_loop(0, rows // (2 * step), go, 0)

    def keys_of(layer):
        keys = jnp.dot(ns[...], wk[layer], preferred_element_type=F32)
        return (keys * row_scale(keys)).astype(BF16)

    def values_of(layer):
        return jnp.dot(ns[...], wv[layer], preferred_element_type=F32).astype(BF16)

    def queries_of(layer):
        hidden = hid[...]
        normed = (hidden * row_scale(hidden) * tgain[layer : layer + 1, :]).astype(BF16)
        queries = jnp.dot(normed, wq[layer], preferred_element_type=F32)
        return (queries * row_scale(queries)).astype(BF16)

    def push(src_ref, dst_ref, send, recv, peer):
        return pltpu.make_async_remote_copy(
            src_ref=src_ref,
            dst_ref=dst_ref,
            send_sem=send,
            recv_sem=recv,
            device_id=peer,
            device_id_type=MESH,
        )

    sign = 1 - 2 * lax.rem(t, 2)
    ahead, behind = lax.rem(y + sign + ny, ny), lax.rem(y - sign + ny, ny)

    def near(which, held, lands):
        return push(
            kv0.at[which, held],
            kv0.at[which, lands],
            kv0_send.at[which, lands],
            kv0_recv.at[which, lands],
            {"y": ahead if lands == 3 else behind},
        )

    right, left = line(1), line(-1)

    def ring(which, step):
        copies = []
        for way, peer in ((0, right), (1, left)):
            if step == half - 1 and which != way:
                continue
            held = 0 if step == 0 else (step if way == 0 else half + step)
            lands = half if step == half - 1 else (step + 1 if way == 0 else half + step + 1)
            copies.append(
                push(
                    kv1.at[which, held],
                    kv1.at[which, lands],
                    kv1_send.at[which, way, step],
                    kv1_recv.at[which, lands],
                    {"y": peer},
                )
            )
        return copies

    def ring_next(step):
        for which in (0, 1):
            for copy in ring(which, step):
                copy.wait_recv()
            if step < half - 1:
                for copy in ring(which, step + 1):
                    copy.start()

    def z_order(i):
        away = (i + 1) // 2
        return lax.rem(nz // 2 + jnp.where(lax.rem(i, 2) == 1, away, -away), nz)

    def q0_start():
        def go(i, carry):
            k = z_order(i)
            for d in range(2):
                push(
                    q0.at[2, 0],
                    q0.at[d, lax.rem(nz - k, nz)],
                    q_send.at[0],
                    q_recv.at[0],
                    {"z": plane(k), "y": line(sides[d])},
                ).start()
            return carry

        lax.fori_loop(0, nz, go, 0)

    def n0_start(d):
        def go(i, carry):
            k = z_order(i)
            push(
                nsend0.at[d, k],
                nrecv0.at[d, lax.rem(nz - k, nz)],
                n_send.at[0],
                n_recv.at[0],
                {"z": plane(k), "y": line(-sides[d])},
            ).start()
            return carry

        lax.fori_loop(0, nz, go, 0)

    def q1_start():
        def go(i, carry):
            k = z_order(i)
            push(q1.at[0], q1.at[nz - k], q_send.at[1], q_recv.at[1], {"z": plane(k)}).start()
            return carry

        lax.fori_loop(0, nz - 1, go, 0)

    def n1_start():
        def go(i, carry):
            k = z_order(i)
            push(
                nsend1.at[k], nrecv1.at[nz - k], n_send.at[1], n_recv.at[1], {"z": plane(k)}
            ).start()
            return carry

        lax.fori_loop(0, nz - 1, go, 0)

    def t_start(layer):
        for k in sorted(range(1, nt), key=lambda k: abs(k - nt // 2)):
            push(
                share.at[layer, 0],
                share.at[layer, nt - k],
                t_send.at[layer],
                t_recv.at[layer],
                {"tp": lax.rem(t + k, nt)},
            ).start()

    waits = []

    def wait_all(ref, send, recv, peer):
        both = push(ref, ref, send, recv, peer)
        both.wait_recv()
        waits.append(both)

    def weigh(layer, queries, keys):
        scores = dot_nt(queries, keys)
        weights = jnp.exp(scl[layer] * (scores * (1.0 / ROOT) - ROOT))
        sums = weights[:, 0:128]
        for c in range(128, weights.shape[1], 128):
            sums = sums + weights[:, c : c + 128]
        return weights.astype(BF16), sums

    def with_denominators(numer, sums):
        denoms = jnp.sum(sums.T, axis=0, keepdims=True)
        upper = denoms.astype(BF16).astype(F32)
        lower = denoms - upper
        pad = jnp.zeros((1, 128 - tall), F32)
        parts = [upper, lower] if tall == 128 else [upper, pad, lower, pad]
        extra = jnp.concatenate(parts, axis=1).reshape(1, 1, 256)
        shape = (nz, PAD, HEAD_DIM)
        lane = lax.rem(lax.broadcasted_iota(jnp.int32, shape, 2), 128)
        block = lax.broadcasted_iota(jnp.int32, shape, 0)
        row = lax.broadcasted_iota(jnp.int32, shape, 1)
        mine = jnp.where(lane // PAD == block, jnp.broadcast_to(extra, shape), 0.0)
        return jnp.where(row == PAD - 1, mine, numer.reshape(shape)).astype(BF16)

    def share_of(layer, total):
        shape = (PAD, 128)
        lane = lax.broadcasted_iota(jnp.int32, shape, 1)
        row = lax.broadcasted_iota(jnp.int32, shape, 0)
        both = total[PAD - 1 : PAD, 0:128] + total[PAD - 1 : PAD, 128:256]
        denoms = jnp.sum(
            jnp.where(lax.rem(lane, PAD) == row, jnp.broadcast_to(both, shape), 0.0),
            axis=1,
            keepdims=True,
        )
        real = lax.broadcasted_iota(jnp.int32, (PAD, HEAD_DIM), 0) < toks
        attended = jnp.where(real, total / denoms, 0.0).astype(BF16)
        share[layer, 0] = jnp.dot(attended, wo[layer], preferred_element_type=F32).astype(BF16)

    def add_branch(layer):
        branch = share[layer, 0].astype(F32)
        for k in range(1, nt):
            branch = branch + share[layer, k].astype(F32)
        return (hid[...] + branch).astype(BF16)

    with scope("load"):
        first[0].wait()
    with scope("norm"):
        lax.fori_loop(0, rows // (2 * step), squares, 0)
        mean = jnp.sum(scale_of[...], axis=-1, keepdims=True) * (1.0 / src.shape[1])
        scale_of[...] = jnp.broadcast_to(lax.rsqrt(mean + EPS), scale_of.shape)
        first[1].wait()
        norm_rows(0)
    with scope("keys_0"):
        first[2].wait()
        kv0[0, 0] = keys_of(0)
    with scope("barrier"):
        pl.semaphore_wait(barrier, greeted)
    near(0, 0, 1).start()
    near(0, 0, 3).start()
    with scope("values_0"):
        first[3].wait()
        kv0[1, 0] = values_of(0)
    near(1, 0, 1).start()
    near(1, 0, 3).start()
    with scope("queries_0"):
        for i in (0, 1, 2):
            later[i].wait()
        hid[...] = jnp.zeros_like(hid)
        hid[0:toks, :] = tgt[...].astype(F32)
        q0[2, 0] = queries_of(0)
        q0_start()
    with scope("source_1"):
        norm_rows(1)
        for i in (3, 4, 5):
            later[i].wait()
        kv1[0, 0] = keys_of(1)
        kv1[1, 0] = values_of(1)
        for i in (6, 7, 8):
            later[i].wait()
    for which in (0, 1):
        with scope(f"near_0_{which}"):
            near(which, 0, 1).wait_recv()
            near(which, 1, 2).start()
            near(which, 0, 3).wait_recv()
    for which in (0, 1):
        for copy in ring(which, 0):
            copy.start()
    with scope("q_wait_0"):
        wait_all(
            q0.at[pl.ds(0, 2)], q_send.at[0], q_recv.at[0], {"z": plane(1), "y": line(2)}
        )
    numer = jnp.zeros((2 * tall, HEAD_DIM), F32)
    total = jnp.zeros((2 * tall, 128), F32)
    queries = q0[0:2].reshape(2 * tall, HEAD_DIM)
    for slot in (0, 1, 3, 2):
        if slot == 2:
            with scope("near_1_0"):
                near(0, 1, 2).wait_recv()
        with scope(f"attend_0_{slot}"):
            weights, sums = weigh(0, queries, kv0[0, slot])
            total = total + sums
        if slot == 2:
            with scope("near_1_1"):
                near(1, 1, 2).wait_recv()
        numer = numer + jnp.dot(weights, kv0[1, slot], preferred_element_type=F32)
    with scope("partials_0"):
        for d in range(2):
            at = slice(d * tall, (d + 1) * tall)
            nsend0[d] = with_denominators(numer[at], total[at])
            n0_start(d)
    with scope("ring_1_0"):
        ring_next(0)
    with scope("ring_1_1"):
        ring_next(1)
    with scope("n_wait_0"):
        wait_all(nrecv0, n_send.at[0], n_recv.at[0], {"z": plane(1), "y": line(2)})
    with scope("share_0"):
        share_of(0, jnp.sum(nrecv0[...].reshape(2 * nz, PAD, HEAD_DIM).astype(F32), axis=0))
        t_start(0)
    with scope("ring_1_2"):
        ring_next(2)
    with scope("t_wait_0"):
        others = {"tp": lax.rem(t + 1, nt)}
        wait_all(share.at[0, pl.ds(1, nt - 1)], t_send.at[0], t_recv.at[0], others)
    with scope("queries_1"):
        hid[...] = add_branch(0).astype(F32)
        q1[0] = queries_of(1)
        q1_start()
    with scope("ring_1_3"):
        ring_next(3)
    with scope("q_wait_1"):
        wait_all(q1.at[pl.ds(1, nz - 1)], q_send.at[1], q_recv.at[1], {"z": plane(1)})
    with scope("attend_1"):
        numer = jnp.zeros((tall, HEAD_DIM), F32)
        total = jnp.zeros((tall, 128), F32)
        queries = q1[...].reshape(tall, HEAD_DIM)
        for slot in range(0, ny, 2):
            keys = kv1[0, slot : slot + 2].reshape(2 * rows, HEAD_DIM)
            weights, sums = weigh(1, queries, keys)
            total = total + sums
            values = kv1[1, slot : slot + 2].reshape(2 * rows, HEAD_DIM)
            numer = numer + jnp.dot(weights, values, preferred_element_type=F32)
    with scope("partials_1"):
        full = with_denominators(numer, total)
        nsend1[...] = full
        nrecv1[0] = full[0]
        n1_start()
    with scope("n_wait_1"):
        wait_all(nrecv1.at[pl.ds(1, nz - 1)], n_send.at[1], n_recv.at[1], {"z": plane(1)})
    with scope("share_1"):
        share_of(1, jnp.sum(nrecv1[...].astype(F32), axis=0))
        t_start(1)
    with scope("t_wait_1"):
        wait_all(share.at[1, pl.ds(1, nt - 1)], t_send.at[1], t_recv.at[1], others)
    with scope("drain"):
        out[...] = add_branch(1)[0:toks, :]
        for both in waits:
            both.wait_send()
        for which in (0, 1):
            for held, lands in ((0, 1), (0, 3), (1, 2)):
                near(which, held, lands).wait_send()
            for s in range(half):
                for copy in ring(which, s):
                    copy.wait_send()


def body(sizes, *arrays):
    target, source = arrays[0], arrays[1]
    w_query = arrays[4]
    arrays = (*arrays[:8], arrays[8].reshape(-1))
    nz, ny, nt = sizes
    toks, width = target.shape
    rows = source.shape[0]
    layers = w_query.shape[0]
    half = ny // 2
    hbm = pl.BlockSpec(memory_space=pl.ANY)
    vmem = pltpu.VMEM
    dma = pltpu.SemaphoreType.DMA
    return pl.pallas_call(
        functools.partial(kernel, sizes),
        out_shape=jax.ShapeDtypeStruct((toks, width), BF16),
        in_specs=[hbm] * 9,
        out_specs=pl.BlockSpec(memory_space=pltpu.VMEM),
        scratch_shapes=[
            vmem((PAD, width), F32),
            vmem((rows, width), BF16),
            vmem((rows, 128), F32),
            vmem((toks, width), BF16),
            vmem((layers, width), F32),
            vmem((layers, width), F32),
            vmem((layers, width, HEAD_DIM), BF16),
            vmem((layers, width, HEAD_DIM), BF16),
            vmem((layers, width, HEAD_DIM), BF16),
            vmem((layers, HEAD_DIM, width), BF16),
            pltpu.SMEM((layers,), F32),
            vmem((rows, width), BF16),
            vmem((2, 4, rows, HEAD_DIM), BF16),
            vmem((2, ny, rows, HEAD_DIM), BF16),
            vmem((3, nz, PAD, HEAD_DIM), BF16),
            vmem((nz, PAD, HEAD_DIM), BF16),
            vmem((2, nz, PAD, HEAD_DIM), BF16),
            vmem((2, nz, PAD, HEAD_DIM), BF16),
            vmem((nz, PAD, HEAD_DIM), BF16),
            vmem((nz, PAD, HEAD_DIM), BF16),
            vmem((layers, nt, PAD, width), BF16),
            dma((13,)),
            dma((2, 4)),
            dma((2, 4)),
            dma((2, 2, half)),
            dma((2, ny)),
            dma((layers,)),
            dma((layers,)),
            dma((layers,)),
            dma((layers,)),
            dma((layers,)),
            dma((layers,)),
        ],
        compiler_params=pltpu.CompilerParams(collective_id=0, has_side_effects=True),
    )(*arrays)


SP = ("z", "y")


def torus_of(mesh):
    return Mesh(mesh.devices.reshape(16, 8, mesh.shape["tp"]), ("z", "y", "tp"))


def on_torus(torus):
    sizes = tuple(torus.shape[a] for a in ("z", "y", "tp"))
    return jax.shard_map(
        functools.partial(body, sizes),
        mesh=torus,
        in_specs=(
            P(SP, None),
            P(SP, None),
            P(),
            P(),
            P(None, None, "tp"),
            P(None, None, "tp"),
            P(None, None, "tp"),
            P(None, "tp", None),
            P(None, "tp"),
        ),
        out_specs=P(SP, None),
        check_vma=False,
    )


def solution(mesh):
    return on_torus(torus_of(mesh))
```

time: 88.9 us -> 83.1 us (0.935)
  Pallas kernels: 86 us -> 81.5 us
  local copies, waits for them, and re-layouts: 2.67 us -> 1.38 us
    pallas_call x1, Pallas kernels: 86 us -> 81.5 us  [body(): pl.pallas_call(functools.partial(kernel, sizes), out_shape=jax.ShapeDtype...]
    unnamed x2 -> x1, local copies, waits for them, and re-layouts: 2.67 us -> 1.38 us
where the time goes in v2:
time: 83.1 us; the launch traced here: 82.9 us
  Pallas kernels  81.5 us (98%)
  local copies, waits for them, and re-layouts  1.38 us (2%)
    pallas_call x1, Pallas kernels, body(): pl.pallas_call(functools.partial(kernel, sizes), out_shape=jax.ShapeDtype...  81.5 us

profile of v2, /device:TPU:1, one launch (start us, length us, event | category | flops | bytes accessed | tf_op | source)
XLA Modules:
  0.0 82.9 jit_solution(6545261924550875842)
XLA Ops:
  0.0 81.5 %shard_map.91 = bf16[7,2048]{1,0:T(8,128)(2,1)} custom-call(bf16[7,2048]{1,0:T(8,128)(2,1)} %target.1, bf16[256,2048]{1,0:T(8,128)(2,1)} %source.1, f32[2,2048]{1,0:T(2,128)} %tgt_gain.1, f32[2,2048]{1,0:T(2,128)} %src_gain.1, bf16[2,2048,256]{2,1,0:T(8,128)(2,1)} %w_query.1, bf16[2,2048,256]{2,1,0:T(8,128)(2,1)} %w_key.1, bf16[2,2048,256]{2,1,0:T(8,128)(2,1)} %w_value.1, ...), custom_call_target="tpu_custom_call" | custom-call | tf_op jit(solution)/shard_map/pallas_call | solution.py:466
  81.5 1.4 %copy.11 = bf16[7,2048]{1,0:T(8,128)(2,1)} copy(bf16[7,2048]{1,0:T(8,128)(2,1)} %shard_map.91) | data formatting | bytes 57344

commit v3 on v2

v3 whole, which is shorter than its diff:
```python
import functools
import math

import jax
import jax.numpy as jnp
from jax import lax
from jax.experimental import pallas as pl
from jax.experimental.pallas import tpu as pltpu
from jax.sharding import Mesh
from jax.sharding import PartitionSpec as P

HEAD_DIM = 256
ROOT = math.sqrt(HEAD_DIM)
EPS = 1e-06
PAD = 8
MESH = pl.DeviceIdType.MESH
scope = jax.named_scope
BF16 = jnp.bfloat16
F32 = jnp.float32


def row_scale(values):
    return lax.rsqrt(jnp.mean(values * values, axis=-1, keepdims=True) + EPS)


def dot_nt(a, b):
    return lax.dot_general(a, b, (((1,), (1,)), ((), ())), preferred_element_type=F32)


def kernel(
    sizes,
    target,
    source,
    tgt_gain,
    src_gain,
    w_query,
    w_key,
    w_value,
    w_out,
    score_scale,
    out,
    hid,
    src,
    scale_of,
    tgt,
    tgain,
    sgain,
    wq,
    wk,
    wv,
    wo,
    scl,
    ns,
    kv0,
    kv1,
    q0,
    q1,
    nsend0,
    nrecv0,
    nsend1,
    nrecv1,
    share,
    halves,
    swap,
    load_sem,
    kv0_send,
    kv0_recv,
    kv1_send,
    kv1_recv,
    q_send,
    q_recv,
    h_send,
    h_recv,
    n0_send,
    n0_recv,
    n1_send,
    n1_recv,
    t_send,
    t_recv,
    s_send,
    s_recv,
):
    nz, ny, nt = sizes
    half = ny // 2
    z, y, t = lax.axis_index("z"), lax.axis_index("y"), lax.axis_index("tp")
    layers = wq.shape[0]
    rows = src.shape[0]
    toks = target.shape[0]
    mid = nz // 2
    groups = ((0, mid), (mid, nz))
    tall = mid * PAD
    width = hid.shape[2]

    def wrapped(i, n):
        return jnp.where(i >= n, i - n, i)

    def line(dy):
        return wrapped(y + (dy % ny), ny)

    def plane(k):
        return wrapped(z + k, nz)

    def other(k):
        return wrapped(t + k, nt)

    core = lax.rem(t, 2)
    partner = {"tp": t + 1 - 2 * core}

    def load(i, a, b):
        return pltpu.make_async_copy(a, b, load_sem.at[i])

    first = [
        load(0, target, tgt),
        load(1, tgt_gain, tgain),
        load(2, w_query.at[0], wq.at[0]),
        load(3, source, src),
        load(4, src_gain, sgain),
        load(5, w_key.at[0], wk.at[0]),
        load(6, w_value.at[0], wv.at[0]),
    ]
    later = [
        load(7, score_scale, scl),
        load(8, w_key.at[1], wk.at[1]),
        load(9, w_value.at[1], wv.at[1]),
        load(10, w_out.at[0], wo.at[0]),
        load(11, w_query.at[1], wq.at[1]),
        load(12, w_out.at[1], wo.at[1]),
    ]
    for one in first:
        one.start()

    barrier = pltpu.get_barrier_semaphore()

    def greet(peer):
        pl.semaphore_signal(barrier, inc=1, device_id=peer, device_id_type=MESH)

    sides = (2, -2)
    for dy in (1, -1) + sides:
        greet({"y": line(dy)})
    for k in range(1, nt):
        greet({"tp": other(k)})

    def far_first(i):
        away = (i + 1) // 2
        return wrapped(mid + jnp.where(lax.rem(i, 2) == 1, away, -away), nz)

    def greet_planes(i, carry):
        k = far_first(i)
        greet({"z": plane(k)})
        for dy in sides:
            greet({"z": plane(k), "y": line(dy)})
        return carry

    lax.fori_loop(0, nz - 1, greet_planes, 0)
    greeted = 4 + nt - 1 + (nz - 1) * 3
    for one in later:
        one.start()

    step = 16

    def at_rows(i):
        return pl.ds(pl.multiple_of(i * step, step), step)

    def both_layers(i, carry):
        for u in range(2):
            at = at_rows(2 * i + u)
            x = src[at, :].astype(F32)
            for layer in range(layers):
                ns[layer, at, :] = (x * sgain[layer : layer + 1, :]).astype(BF16)
            x = x * x
            total = x[:, 0:128]
            for c in range(128, x.shape[1], 128):
                total = total + x[:, c : c + 128]
            scale_of[at, :] = total
        return carry

    def source_scale():
        mean = jnp.sum(scale_of[...], axis=-1, keepdims=True) * (1.0 / src.shape[1])
        return lax.rsqrt(mean + EPS)

    def keys_of(layer):
        keys = jnp.dot(ns[layer], wk[layer], preferred_element_type=F32) * source_scale()
        return (keys * row_scale(keys)).astype(BF16)

    def values_of(layer):
        values = jnp.dot(ns[layer], wv[layer], preferred_element_type=F32) * source_scale()
        return values.astype(BF16)

    def queries_of(layer):
        hidden = jnp.concatenate([hid[0], hid[1]], axis=1)
        normed = (hidden * row_scale(hidden) * tgain[layer : layer + 1, :]).astype(BF16)
        queries = jnp.dot(normed, wq[layer], preferred_element_type=F32)
        return (queries * row_scale(queries)).astype(BF16)

    def push(src_ref, dst_ref, send, recv, peer):
        return pltpu.make_async_remote_copy(
            src_ref=src_ref,
            dst_ref=dst_ref,
            send_sem=send,
            recv_sem=recv,
            device_id=peer,
            device_id_type=MESH,
        )

    sign = 1 - 2 * lax.rem(t, 2)
    ahead, behind = lax.rem(y + sign + ny, ny), lax.rem(y - sign + ny, ny)

    def near(which, held, lands):
        return push(
            kv0.at[which, held],
            kv0.at[which, lands],
            kv0_send.at[which, lands],
            kv0_recv.at[which, lands],
            {"y": ahead if lands == 3 else behind},
        )

    right, left = line(1), line(-1)

    def ring(which, step):
        copies = []
        for way, peer in ((0, right), (1, left)):
            if step == half - 1 and which != way:
                continue
            held = 0 if step == 0 else (step if way == 0 else half + step)
            lands = half if step == half - 1 else (step + 1 if way == 0 else half + step + 1)
            copies.append(
                push(
                    kv1.at[which, held],
                    kv1.at[which, lands],
                    kv1_send.at[which, way, step],
                    kv1_recv.at[which, lands],
                    {"y": peer},
                )
            )
        return copies

    def ring_next(step):
        for which in (0, 1):
            for copy in ring(which, step):
                copy.wait_recv()
            if step < half - 1:
                for copy in ring(which, step + 1):
                    copy.start()

    def hop(d):
        return push(
            q0.at[2, 0],
            q0.at[d, z],
            h_send.at[0, d],
            h_recv.at[0, d],
            {"y": line(sides[d])},
        )

    def q0_straight():
        def go(i, carry):
            for d in range(2):
                push(
                    q0.at[2, 0],
                    q0.at[d, z],
                    q_send.at[0],
                    q_recv.at[0, 0],
                    {"z": plane(far_first(i)), "y": line(sides[d])},
                ).start()
            return carry

        lax.fori_loop(0, nz, go, 0)

    def q0_relay(d):
        def go(i, carry):
            push(
                q0.at[d, z],
                q0.at[d, z],
                q_send.at[0],
                q_recv.at[0, 1],
                {"z": plane(far_first(i))},
            ).start()
            return carry

        lax.fori_loop(0, nz - 1, go, 0)

    def n0_start(g):
        def go(i, carry):
            for d in range(2):
                push(
                    nsend0.at[d, i],
                    nrecv0.at[d, z],
                    n0_send,
                    n0_recv,
                    {"z": i, "y": line(-sides[d])},
                ).start()
            return carry

        lax.fori_loop(*groups[g], go, 0)

    early = z < mid

    def wait_group(layer, g, some_of):
        inside = early if g == 0 else jnp.logical_not(early)
        for less, when in ((1, inside), (0, jnp.logical_not(inside))):

            @pl.when(when)
            def _(less=less):
                some = some_of(mid - less)
                push(some, some, q_send.at[layer], q_recv.at[layer, g], {"z": plane(1)}).wait_recv()

    def q1_start():
        for g, (low, high) in enumerate(groups):

            def go(i, carry):
                @pl.when(i != z)
                def _():
                    push(
                        q1.at[nz], q1.at[z], q_send.at[1], q_recv.at[1, lax.div(z, mid)], {"z": i}
                    ).start()

                return carry

            lax.fori_loop(low, high, go, 0)

    def n1_start(g):
        def go(i, carry):
            @pl.when(i != z)
            def _():
                push(nsend1.at[i], nrecv1.at[z], n1_send, n1_recv, {"z": i}).start()

            return carry

        lax.fori_loop(*groups[g], go, 0)

    def share_start(layer):
        for k in sorted(range(1, nt), key=lambda k: abs(k - nt // 2)):
            push(
                share.at[layer, lax.rem(t + k, 2)],
                halves.at[layer, nt - k],
                t_send.at[layer],
                t_recv.at[layer],
                {"tp": other(k)},
            ).start()

    waits = []

    def wait_all(ref, send, recv, peer):
        both = push(ref, ref, send, recv, peer)
        both.wait_recv()
        waits.append(both)

    def weigh(layer, queries, keys):
        scores = dot_nt(queries, keys)
        weights = jnp.exp(scl[layer] * (scores * (1.0 / ROOT) - ROOT))
        sums = weights[:, 0:128]
        for c in range(128, weights.shape[1], 128):
            sums = sums + weights[:, c : c + 128]
        return weights.astype(BF16), sums

    def with_denominators(numer, sums):
        count = numer.shape[0]
        denoms = jnp.sum(sums.T, axis=0, keepdims=True)
        upper = denoms.astype(BF16).astype(F32)
        parts = [upper, denoms - upper]
        if count < 128:
            pad = jnp.zeros((1, 128 - count), F32)
            parts = [parts[0], pad, parts[1], pad]
        extra = jnp.concatenate(parts, axis=1).reshape(1, 1, 256)
        shape = (count // PAD, PAD, HEAD_DIM)
        lane = lax.rem(lax.broadcasted_iota(jnp.int32, shape, 2), 128)
        block = lax.broadcasted_iota(jnp.int32, shape, 0)
        row = lax.broadcasted_iota(jnp.int32, shape, 1)
        mine = jnp.where(lane // PAD == block, jnp.broadcast_to(extra, shape), 0.0)
        return jnp.where(row == PAD - 1, mine, numer.reshape(shape)).astype(BF16)

    def share_of(layer, total):
        shape = (PAD, 128)
        lane = lax.broadcasted_iota(jnp.int32, shape, 1)
        row = lax.broadcasted_iota(jnp.int32, shape, 0)
        both = total[PAD - 1 : PAD, 0:128] + total[PAD - 1 : PAD, 128:256]
        denoms = jnp.sum(
            jnp.where(lax.rem(lane, PAD) == row, jnp.broadcast_to(both, shape), 0.0),
            axis=1,
            keepdims=True,
        )
        real = lax.broadcasted_iota(jnp.int32, (PAD, HEAD_DIM), 0) < toks
        attended = jnp.where(real, total / denoms, 0.0).astype(BF16)
        rounded = jnp.dot(attended, wo[layer], preferred_element_type=F32).astype(BF16)
        share[layer, 0] = rounded[:, 0:width]
        share[layer, 1] = rounded[:, width : 2 * width]
        share_start(layer)

    def add_branch(layer):
        wait_all(halves.at[layer, pl.ds(1, nt - 1)], t_send.at[layer], t_recv.at[layer], partner)
        branch = share[layer, core].astype(F32)
        for k in range(1, nt):
            branch = branch + halves[layer, k].astype(F32)
        swap[layer, core] = (hid[core] + branch).astype(BF16)
        both = push(
            swap.at[layer, core], swap.at[layer, core], s_send.at[layer], s_recv.at[layer], partner
        )
        both.start()
        both.wait_recv()
        waits.append(both)

    with scope("queries_0"):
        for i in range(3):
            first[i].wait()
        hid[...] = jnp.zeros_like(hid)
        rows_in = tgt[...].astype(F32)
        hid[0, 0:toks, :] = rows_in[:, 0:width]
        hid[1, 0:toks, :] = rows_in[:, width : 2 * width]
        q0[2, 0] = queries_of(0)
    with scope("norm"):
        first[3].wait()
        first[4].wait()
        lax.fori_loop(0, rows // (2 * step), both_layers, 0)
    with scope("keys_0"):
        first[5].wait()
        kv0[0, 0] = keys_of(0)
    with scope("barrier"):
        pl.semaphore_wait(barrier, greeted)

    @pl.when(early)
    def _():
        q0_straight()

    @pl.when(jnp.logical_not(early))
    def _():
        for d in range(2):
            hop(d).start()

    near(0, 0, 1).start()
    near(0, 0, 3).start()
    with scope("values_0"):
        first[6].wait()
        kv0[1, 0] = values_of(0)
    near(1, 0, 1).start()
    near(1, 0, 3).start()
    with scope("source_1"):
        for i in (0, 1, 2):
            later[i].wait()
        kv1[0, 0] = keys_of(1)
        kv1[1, 0] = values_of(1)
        for i in (3, 4, 5):
            later[i].wait()
    with scope("hop_0"):

        @pl.when(jnp.logical_not(early))
        def _():
            for d in range(2):
                hop(d).wait_recv()
                q0_relay(d)

    for which in (0, 1):
        with scope(f"near_0_{which}"):
            near(which, 0, 1).wait_recv()
            near(which, 1, 2).start()
            near(which, 0, 3).wait_recv()
    for g, (low, high) in enumerate(groups):
        with scope(f"q_wait_0_{g}"):
            some = q0.at[pl.ds(0, 2), pl.ds(low, mid)]
            if g == 0:
                push(some, some, q_send.at[0], q_recv.at[0, 0], {"z": plane(1)}).wait_recv()
            else:
                wait_group(0, g, lambda count, low=low: q0.at[pl.ds(0, 2), pl.ds(low, count)])
        numer = jnp.zeros((2 * tall, HEAD_DIM), F32)
        total = jnp.zeros((2 * tall, 128), F32)
        queries = q0[0:2, low:high].reshape(2 * tall, HEAD_DIM)
        for slot in (0, 1, 3, 2):
            if slot == 2 and g == 0:
                for which in (0, 1):
                    with scope(f"near_1_{which}"):
                        near(which, 1, 2).wait_recv()
                        for copy in ring(which, 0):
                            copy.start()
            with scope(f"attend_0_{g}_{slot}"):
                weights, sums = weigh(0, queries, kv0[0, slot])
                total = total + sums
            numer = numer + jnp.dot(weights, kv0[1, slot], preferred_element_type=F32)
        with scope(f"partials_0_{g}"):
            nsend0[:, low:high] = with_denominators(numer, total).reshape(2, mid, PAD, HEAD_DIM)
            n0_start(g)
    with scope("ring_1_0"):
        ring_next(0)
    with scope("ring_late"):

        @pl.when(jnp.logical_not(early))
        def _():
            ring_next(1)
            ring_next(2)

    with scope("n_wait_0"):
        wait_all(nrecv0, n0_send, n0_recv, {"z": plane(1)})
    with scope("share_0"):
        share_of(0, jnp.sum(nrecv0[...].reshape(2 * nz, PAD, HEAD_DIM).astype(F32), axis=0))
    def serve(g):
        low, high = groups[g]
        with scope(f"q_wait_1_{g}"):
            wait_group(1, g, lambda count, low=low: q1.at[pl.ds(low, count)])
        with scope(f"attend_1_{g}"):
            numer = jnp.zeros((tall, HEAD_DIM), F32)
            total = jnp.zeros((tall, 128), F32)
            queries = q1[low:high].reshape(tall, HEAD_DIM)
            for slot in range(0, ny, 2):
                keys = kv1[0, slot : slot + 2].reshape(2 * rows, HEAD_DIM)
                weights, sums = weigh(1, queries, keys)
                total = total + sums
                values = kv1[1, slot : slot + 2].reshape(2 * rows, HEAD_DIM)
                numer = numer + jnp.dot(weights, values, preferred_element_type=F32)
        with scope(f"partials_1_{g}"):
            nsend1[low:high] = with_denominators(numer, total)
            n1_start(g)

    @pl.when(early)
    def _():
        with scope("ring_1_1"):
            ring_next(1)

    @pl.when(jnp.logical_not(early))
    def _():
        with scope("ring_1_3"):
            ring_next(3)
        serve(0)

    with scope("t_wait_0"):
        add_branch(0)
    with scope("queries_1"):
        hid[...] = swap[0].astype(F32)
        own = queries_of(1)
        q1[nz] = own
        q1[z] = own
        q1_start()
    @pl.when(early)
    def _():
        with scope("ring_early"):
            ring_next(2)
            ring_next(3)
        serve(0)

    @pl.when(jnp.logical_not(early))
    def _():
        serve(1)

    with scope("n_wait_1"):
        nrecv1[z] = nsend1[z]
        some = nrecv1.at[pl.ds(0, nz - 1)]
        wait_all(some, n1_send, n1_recv, {"z": plane(1)})
    with scope("share_1"):
        share_of(1, jnp.sum(nrecv1[...].astype(F32), axis=0))

    @pl.when(early)
    def _():
        serve(1)

    with scope("t_wait_1"):
        add_branch(1)
    with scope("drain"):
        out[:, 0:width] = swap[1, 0][0:toks, :]
        out[:, width : 2 * width] = swap[1, 1][0:toks, :]
        for both in waits:
            both.wait_send()

        def sent(layer, some):
            push(
                some, some, q_send.at[layer], q_recv.at[layer, 0], {"z": plane(1)}
            ).wait_send()

        sent(1, q1.at[pl.ds(0, nz - 1)])

        @pl.when(early)
        def _():
            sent(0, q0.at[pl.ds(0, 2)])

        @pl.when(jnp.logical_not(early))
        def _():
            sent(0, q0.at[pl.ds(0, 2), pl.ds(0, nz - 1)])
            for d in range(2):
                hop(d).wait_send()

        for which in (0, 1):
            for held, lands in ((0, 1), (0, 3), (1, 2)):
                near(which, held, lands).wait_send()
            for s in range(half):
                for copy in ring(which, s):
                    copy.wait_send()


def body(sizes, *arrays):
    target, source = arrays[0], arrays[1]
    w_query = arrays[4]
    arrays = (*arrays[:8], arrays[8].reshape(-1))
    nz, ny, nt = sizes
    toks, width = target.shape
    rows = source.shape[0]
    layers = w_query.shape[0]
    half = ny // 2
    hbm = pl.BlockSpec(memory_space=pl.ANY)
    vmem = pltpu.VMEM
    dma = pltpu.SemaphoreType.DMA
    return pl.pallas_call(
        functools.partial(kernel, sizes),
        out_shape=pltpu.VMEM((toks, width), BF16),
        in_specs=[hbm] * 9,
        out_specs=pl.BlockSpec(memory_space=pltpu.VMEM),
        scratch_shapes=[
            vmem((2, PAD, width // 2), F32),
            vmem((rows, width), BF16),
            vmem((rows, 128), F32),
            vmem((toks, width), BF16),
            vmem((layers, width), F32),
            vmem((layers, width), F32),
            vmem((layers, width, HEAD_DIM), BF16),
            vmem((layers, width, HEAD_DIM), BF16),
            vmem((layers, width, HEAD_DIM), BF16),
            vmem((layers, HEAD_DIM, width), BF16),
            pltpu.SMEM((layers,), F32),
            vmem((layers, rows, width), BF16),
            vmem((2, 4, rows, HEAD_DIM), BF16),
            vmem((2, ny, rows, HEAD_DIM), BF16),
            vmem((3, nz, PAD, HEAD_DIM), BF16),
            vmem((nz + 1, PAD, HEAD_DIM), BF16),
            vmem((2, nz, PAD, HEAD_DIM), BF16),
            vmem((2, nz, PAD, HEAD_DIM), BF16),
            vmem((nz, PAD, HEAD_DIM), BF16),
            vmem((nz, PAD, HEAD_DIM), BF16),
            vmem((layers, 2, PAD, width // 2), BF16),
            vmem((layers, nt, PAD, width // 2), BF16),
            vmem((layers, 2, PAD, width // 2), BF16),
            dma((13,)),
            dma((2, 4)),
            dma((2, 4)),
            dma((2, 2, half)),
            dma((2, ny)),
            dma((layers,)),
            dma((layers, 2)),
            dma((1, 2)),
            dma((1, 2)),
            dma,
            dma,
            dma,
            dma,
            dma((layers,)),
            dma((layers,)),
            dma((layers,)),
            dma((layers,)),
        ],
        compiler_params=pltpu.CompilerParams(collective_id=0, has_side_effects=True),
    )(*arrays)


SP = ("z", "y")


def torus_of(mesh):
    return Mesh(mesh.devices.reshape(16, 8, mesh.shape["tp"]), ("z", "y", "tp"))


def on_torus(torus):
    sizes = tuple(torus.shape[a] for a in ("z", "y", "tp"))
    return jax.shard_map(
        functools.partial(body, sizes),
        mesh=torus,
        in_specs=(
            P(SP, None),
            P(SP, None),
            P(),
            P(),
            P(None, None, "tp"),
            P(None, None, "tp"),
            P(None, None, "tp"),
            P(None, "tp", None),
            P(None, "tp"),
        ),
        out_specs=P(SP, None),
        check_vma=False,
    )


def solution(mesh):
    return on_torus(torus_of(mesh))
```

time: 83.1 us -> 77.4 us (0.931)
  Pallas kernels: 81.5 us -> 76.6 us
    pallas_call x1, Pallas kernels: 81.5 us -> 76.6 us  [body(): pl.pallas_call(functools.partial(kernel, sizes), out_shape=pltpu.VMEM((to...]
where the time goes in v3:
time: 77.4 us; the launch traced here: 77.2 us
  Pallas kernels  76.6 us (99%)
    pallas_call x1, Pallas kernels, body(): pl.pallas_call(functools.partial(kernel, sizes), out_shape=pltpu.VMEM((to...  76.6 us

profile of v3, /device:TPU:1, one launch (start us, length us, event | category | flops | bytes accessed | tf_op | source)
XLA Modules:
  0.0 77.2 jit_solution(5462520703793389736)
XLA Ops:
  0.0 76.6 %shard_map.91 = bf16[7,2048]{1,0:T(8,128)(2,1)S(1)} custom-call(bf16[7,2048]{1,0:T(8,128)(2,1)} %target.1, bf16[256,2048]{1,0:T(8,128)(2,1)} %source.1, f32[2,2048]{1,0:T(2,128)} %tgt_gain.1, f32[2,2048]{1,0:T(2,128)} %src_gain.1, bf16[2,2048,256]{2,1,0:T(8,128)(2,1)} %w_query.1, bf16[2,2048,256]{2,1,0:T(8,128)(2,1)} %w_key.1, ...), custom_call_target="tpu_custom_call" | custom-call | tf_op jit(solution)/shard_map/pallas_call | solution.py:596
  76.6 0.6 copy.11

commit v4 on v3

--- a/solution.py
+++ b/solution.py
@@ -60,6 +60,9 @@
     nsend1,
     nrecv1,
     share,
+    back_send,
+    back_recv,
+    gathered,
     halves,
     swap,
     load_sem,
@@ -71,6 +74,8 @@
     q_recv,
     h_send,
     h_recv,
+    b_send,
+    b_recv,
     n0_send,
     n0_recv,
     n1_send,
@@ -278,7 +283,7 @@
 
         lax.fori_loop(0, nz - 1, go, 0)
 
-    def n0_start(g):
+    def n0_straight():
         def go(i, carry):
             for d in range(2):
                 push(
@@ -290,7 +295,29 @@
                 ).start()
             return carry
 
-        lax.fori_loop(*groups[g], go, 0)
+        lax.fori_loop(*groups[0], go, 0)
+
+    def n0_along():
+        def go(i, carry):
+            @pl.when(i != z)
+            def _():
+                for d in range(2):
+                    push(
+                        nsend0.at[d, i], nrecv0.at[d, z], n0_send, n0_recv, {"z": i}
+                    ).start()
+
+            return carry
+
+        lax.fori_loop(*groups[1], go, 0)
+
+    def back(d):
+        return push(
+            back_send.at[d],
+            back_recv.at[d],
+            b_send.at[d],
+            b_recv.at[d],
+            {"y": line(-sides[d])},
+        )
 
     early = z < mid
 
@@ -475,20 +502,35 @@
             numer = numer + jnp.dot(weights, kv0[1, slot], preferred_element_type=F32)
         with scope(f"partials_0_{g}"):
             nsend0[:, low:high] = with_denominators(numer, total).reshape(2, mid, PAD, HEAD_DIM)
-            n0_start(g)
+            n0_straight() if g == 0 else n0_along()
     with scope("ring_1_0"):
         ring_next(0)
     with scope("ring_late"):
 
         @pl.when(jnp.logical_not(early))
         def _():
+            some = nrecv0.at[pl.ds(0, 2), pl.ds(0, nz - 1)]
+            push(some, some, n0_send, n0_recv, {"z": plane(1)}).wait_recv()
+            for d in range(2):
+                nrecv0[d, z] = nsend0[d, z]
+                back_send[d] = jnp.sum(nrecv0[d].astype(F32), axis=0)
+                back(d).start()
             ring_next(1)
-            ring_next(2)
+            for d in range(2):
+                back(d).wait_recv()
+            gathered[...] = back_recv[0] + back_recv[1]
 
     with scope("n_wait_0"):
-        wait_all(nrecv0, n0_send, n0_recv, {"z": plane(1)})
+
+        @pl.when(early)
+        def _():
+            push(nrecv0, nrecv0, n0_send, n0_recv, {"z": plane(1)}).wait_recv()
+            gathered[...] = jnp.sum(
+                nrecv0[...].reshape(2 * nz, PAD, HEAD_DIM).astype(F32), axis=0
+            )
+
     with scope("share_0"):
-        share_of(0, jnp.sum(nrecv0[...].reshape(2 * nz, PAD, HEAD_DIM).astype(F32), axis=0))
+        share_of(0, gathered[...])
     def serve(g):
         low, high = groups[g]
         with scope(f"q_wait_1_{g}"):
@@ -514,9 +556,8 @@
 
     @pl.when(jnp.logical_not(early))
     def _():
-        with scope("ring_1_3"):
-            ring_next(3)
-        serve(0)
+        with scope("ring_1_2"):
+            ring_next(2)
 
     with scope("t_wait_0"):
         add_branch(0)
@@ -528,26 +569,18 @@
         q1_start()
     @pl.when(early)
     def _():
-        with scope("ring_early"):
-            ring_next(2)
-            ring_next(3)
-        serve(0)
-
-    @pl.when(jnp.logical_not(early))
-    def _():
-        serve(1)
-
+        ring_next(2)
+
+    with scope("ring_1_3"):
+        ring_next(3)
+    serve(0)
+    serve(1)
     with scope("n_wait_1"):
         nrecv1[z] = nsend1[z]
         some = nrecv1.at[pl.ds(0, nz - 1)]
         wait_all(some, n1_send, n1_recv, {"z": plane(1)})
     with scope("share_1"):
         share_of(1, jnp.sum(nrecv1[...].astype(F32), axis=0))
-
-    @pl.when(early)
-    def _():
-        serve(1)
-
     with scope("t_wait_1"):
         add_branch(1)
     with scope("drain"):
@@ -566,12 +599,16 @@
         @pl.when(early)
         def _():
             sent(0, q0.at[pl.ds(0, 2)])
+            push(nrecv0, nrecv0, n0_send, n0_recv, {"z": plane(1)}).wait_send()
 
         @pl.when(jnp.logical_not(early))
         def _():
             sent(0, q0.at[pl.ds(0, 2), pl.ds(0, nz - 1)])
             for d in range(2):
                 hop(d).wait_send()
+                back(d).wait_send()
+            some = nsend0.at[pl.ds(0, 2), pl.ds(0, nz - 1)]
+            push(some, some, n0_send, n0_recv, {"z": plane(1)}).wait_send()
 
         for which in (0, 1):
             for held, lands in ((0, 1), (0, 3), (1, 2)):
@@ -620,6 +657,9 @@
             vmem((nz, PAD, HEAD_DIM), BF16),
             vmem((nz, PAD, HEAD_DIM), BF16),
             vmem((layers, 2, PAD, width // 2), BF16),
+            vmem((2, PAD, HEAD_DIM), F32),
+            vmem((2, PAD, HEAD_DIM), F32),
+            vmem((PAD, HEAD_DIM), F32),
             vmem((layers, nt, PAD, width // 2), BF16),
             vmem((layers, 2, PAD, width // 2), BF16),
             dma((13,)),
@@ -631,6 +671,8 @@
             dma((layers, 2)),
             dma((1, 2)),
             dma((1, 2)),
+            dma((2,)),
+            dma((2,)),
             dma,
             dma,
             dma,

time: 77.4 us -> 77.1 us (level)
  no operation moved by 1% of the time
where the time goes in v4:
time: 77.1 us; the launch traced here: 77 us
  Pallas kernels  76.4 us (99%)
    pallas_call x1, Pallas kernels, body(): pl.pallas_call(functools.partial(kernel, sizes), out_shape=pltpu.VMEM((to...  76.4 us

profile of v4, /device:TPU:1, one launch (start us, length us, event | category | flops | bytes accessed | tf_op | source)
XLA Modules:
  0.0 77.0 jit_solution(14266934102750149258)
XLA Ops:
  0.0 76.4 %shard_map.91 = bf16[7,2048]{1,0:T(8,128)(2,1)S(1)} custom-call(bf16[7,2048]{1,0:T(8,128)(2,1)} %target.1, bf16[256,2048]{1,0:T(8,128)(2,1)} %source.1, f32[2,2048]{1,0:T(2,128)} %tgt_gain.1, f32[2,2048]{1,0:T(2,128)} %src_gain.1, bf16[2,2048,256]{2,1,0:T(8,128)(2,1)} %w_query.1, bf16[2,2048,256]{2,1,0:T(8,128)(2,1)} %w_key.1, ...), custom_call_target="tpu_custom_call" | custom-call | tf_op jit(solution)/shard_map/pallas_call | solution.py:633
  76.4 0.6 copy.11

commit v5 on v4

--- a/solution.py
+++ b/solution.py
@@ -331,18 +331,17 @@
                 push(some, some, q_send.at[layer], q_recv.at[layer, g], {"z": plane(1)}).wait_recv()
 
     def q1_start():
-        for g, (low, high) in enumerate(groups):
-
-            def go(i, carry):
-                @pl.when(i != z)
-                def _():
-                    push(
-                        q1.at[nz], q1.at[z], q_send.at[1], q_recv.at[1, lax.div(z, mid)], {"z": i}
-                    ).start()
-
-                return carry
-
-            lax.fori_loop(low, high, go, 0)
+        def go(i, carry):
+            push(
+                q1.at[nz],
+                q1.at[z],
+                q_send.at[1],
+                q_recv.at[1, lax.div(z, mid)],
+                {"z": plane(far_first(i))},
+            ).start()
+            return carry
+
+        lax.fori_loop(0, nz - 1, go, 0)
 
     def n1_start(g):
         def go(i, carry):

time: 77.1 us -> 77.1 us (level)
  no operation moved by 1% of the time
where the time goes in v5:
time: 77.1 us; the launch traced here: 77 us
  Pallas kernels  76.4 us (99%)
    pallas_call x1, Pallas kernels, body(): pl.pallas_call(functools.partial(kernel, sizes), out_shape=pltpu.VMEM((to...  76.4 us

profile of v5, /device:TPU:1, one launch (start us, length us, event | category | flops | bytes accessed | tf_op | source)
XLA Modules:
  0.0 77.0 jit_solution(9087927551732114103)
XLA Ops:
  0.0 76.4 %shard_map.91 = bf16[7,2048]{1,0:T(8,128)(2,1)S(1)} custom-call(bf16[7,2048]{1,0:T(8,128)(2,1)} %target.1, bf16[256,2048]{1,0:T(8,128)(2,1)} %source.1, f32[2,2048]{1,0:T(2,128)} %tgt_gain.1, f32[2,2048]{1,0:T(2,128)} %src_gain.1, bf16[2,2048,256]{2,1,0:T(8,128)(2,1)} %w_query.1, bf16[2,2048,256]{2,1,0:T(8,128)(2,1)} %w_key.1, ...), custom_call_target="tpu_custom_call" | custom-call | tf_op jit(solution)/shard_map/pallas_call | solution.py:632
  76.4 0.6 copy.11
